TPU v7x, 32 devices: a whole 2x2x4 slice. The times are simulated.
32 devices in a mesh: ep: 8 (over z, core), tp: 4 (over y, x).
Axes of the slice: x: 2, y: 2, z: 4, core: 2. Of those that a mesh axis runs over, the one named last changes fastest.
Arguments:
- mixer_rows: bfloat16 [4096, 2048], P('ep', 'tp'), may hold values from -6 to 6
- expert_rows: bfloat16 [4096, 2048], P('ep', 'tp'), may hold values from -6 to 6
- mixer_gain: float32 [2048], replicated, may hold values from 0.1 to 1.9
- pool_scale: float32 [2048], P('tp'), may hold values from 0.1 to 1.9
- w_in: bfloat16 [2048, 2048], P(None, 'tp'), may hold values from -0.125 to 0.125
- w_mix_out: bfloat16 [2048, 2048], P(None, 'tp'), may hold values from -0.125 to 0.125
- expert_gain: float32 [2048], replicated, may hold values from 0.1 to 1.9
- expert_gate: bfloat16 [8, 2048, 2048], P('ep', None, 'tp'), may hold values from -0.125 to 0.125
- expert_up: bfloat16 [8, 2048, 2048], P('ep', None, 'tp'), may hold values from -0.125 to 0.125
- expert_down: bfloat16 [8, 2048, 2048], P('ep', None, 'tp'), may hold values from -0.125 to 0.125
- routes: int32 [4096, 2], P('ep'), may hold values from 0 to 7, all different within a row; in each aligned block of 512 rows (0 to 511, 512 to 1023, ...) at most 192 rows name the same one
- route_weight: float32 [4096, 2], P('ep'), may hold values from 0.1 to 1
Outputs:
- mixer_output: bfloat16 [4096, 2048], P('ep', 'tp')
- expert_output: bfloat16 [4096, 2048], P('ep', 'tp')
Inputs may be any that keep to these rules, and one draw needn't show every extreme that they name: `routes`: each row names 2 different experts. Among the rows of one device (aligned blocks of 512 rows) no expert is named more than 192 times, a bound that some block reaches.
All inputs are finite; a program needn't handle non-finite values.
Results may differ from a plain program's by a relative error of at most 0.0071.
Values may be sent and summed in bfloat16 or wider, within the bound.
No kernel may reach another device: no remote copies, remote signals or barrier semaphores. Data moves between devices by JAX's collectives and lax.ppermute only.
A program may use at most 64 MiB of HBM per device.

v0:
```python
import jax
import jax.numpy as jnp
from jax import lax
from jax.sharding import PartitionSpec as P

PW = 2048
TOP = 2
norm_eps = 1e-05
pool_windows = (2, 4, 8, 16)
rim_rows = 8


def extended_2(block, sides, width):
    for axis, dim in sides:
        count = lax.axis_size(axis)
        forward = [(i, i + 1) for i in range(count - 1)]
        backward = [(target, source) for source, target in forward]
        low = lax.ppermute(
            lax.slice_in_dim(block, block.shape[dim] - width, None, axis=dim), axis, forward
        )
        high = lax.ppermute(lax.slice_in_dim(block, 0, width, axis=dim), axis, backward)
        block = jnp.concatenate([low, block, high], axis=dim)
    return block


def layer_norm(row_block, gain_vec):
    values = row_block.astype(jnp.float32)
    center = values - jnp.mean(values, axis=-1, keepdims=True)
    spread = jnp.mean(center * center, axis=-1, keepdims=True)
    return (center * lax.rsqrt(spread + norm_eps) * gain_vec).astype(jnp.bfloat16)


def pooled_channels(inner_t, scale_local, ep_size, ep_index, tp_index):
    extended = extended_2(inner_t, (("ep", 1),), rim_rows).astype(jnp.float32)
    values = inner_t.astype(jnp.float32)
    channels = values.shape[0]
    row_count = values.shape[1]
    seq_len = row_count * ep_size
    position = ep_index * row_count + jnp.arange(row_count, dtype=jnp.int32)
    channel = tp_index * channels + jnp.arange(channels, dtype=jnp.int32)
    group = channel // (PW // 4)
    running = jnp.zeros((channels, row_count), jnp.float32)
    result = jnp.zeros((channels, row_count), jnp.float32)
    last_half = 0
    for group_id, window in enumerate(pool_windows):
        half_span = window // 2
        for offset in list(range(-half_span, -last_half)) + list(range(last_half, half_span)):
            running = running + extended[:, rim_rows + offset : rim_rows + offset + row_count]
        last_half = half_span
        lower_end = jnp.clip(position - half_span, 0, seq_len)
        upper_end = jnp.clip(position - half_span + window, 0, seq_len)
        counts = (upper_end - lower_end).astype(jnp.float32)
        member = (group == group_id)[:, None]
        result = jnp.where(member, running / counts[None, :], result)
    return ((result - values) * scale_local[:, None]).astype(jnp.bfloat16)


def on_device(
    mixer_rows,
    expert_rows,
    mixer_gain,
    pool_scale,
    w_in,
    w_mix_out,
    expert_gain,
    expert_gate,
    expert_up,
    expert_down,
    routes,
    route_weight,
):
    ep_size = lax.axis_size("ep")
    ep_index = lax.axis_index("ep")
    tp_index = lax.axis_index("tp")
    row_count = routes.shape[0]
    capacity = (3 * TOP * row_count + 2 * ep_size - 1) // (2 * ep_size)
    flat_route = routes.reshape(-1)
    onehot = (flat_route[:, None] == jnp.arange(ep_size, dtype=jnp.int32)[None, :]).astype(
        jnp.int32
    )
    ranking = jnp.sum(onehot * (jnp.cumsum(onehot, axis=0) - 1), axis=1)
    target = flat_route * capacity + ranking
    sender = (
        jnp.zeros((ep_size * capacity,), jnp.int32)
        .at[target]
        .set(jnp.arange(row_count * TOP, dtype=jnp.int32) // TOP + 1)
    )
    filled = (sender > 0)[:, None]
    source_row = jnp.maximum(sender - 1, 0)
    full_mix = lax.all_gather(mixer_rows, "tp", axis=1, tiled=True)
    feature_count = expert_rows.shape[1]
    outgoing = jnp.where(filled, expert_rows[source_row], jnp.zeros((), jnp.bfloat16))
    arrived = lax.all_to_all(
        outgoing.reshape(ep_size, capacity, feature_count),
        "ep",
        split_axis=0,
        concat_axis=0,
        tiled=True,
    )
    slot_slices = arrived.reshape(ep_size * capacity, feature_count)
    slot_normed = layer_norm(lax.all_gather(slot_slices, "tp", axis=1, tiled=True), expert_gain)
    contract_first = (((0,), (1,)), ((), ()))
    normed_mix = layer_norm(full_mix, mixer_gain)
    inner_t = lax.dot_general(
        w_in, normed_mix, contract_first, preferred_element_type=jnp.float32
    ).astype(jnp.bfloat16)
    pooled_t = pooled_channels(inner_t, pool_scale, ep_size, ep_index, tp_index)
    gate_t = lax.dot_general(
        expert_gate[0], slot_normed, contract_first, preferred_element_type=jnp.float32
    )
    up_t = lax.dot_general(
        expert_up[0], slot_normed, contract_first, preferred_element_type=jnp.float32
    )
    hidden_t = (jax.nn.silu(gate_t) * up_t).astype(jnp.bfloat16)
    contract_lead = (((0,), (0,)), ((), ()))
    down_weight = expert_down[0]
    mixed_sum = lax.dot_general(
        lax.all_gather(pooled_t, "tp", axis=0, tiled=True),
        w_mix_out,
        contract_lead,
        preferred_element_type=jnp.float32,
    )
    expert_sum = lax.dot_general(
        lax.all_gather(hidden_t, "tp", axis=0, tiled=True),
        down_weight,
        contract_lead,
        preferred_element_type=jnp.float32,
    )
    mixer_output = mixed_sum.astype(jnp.bfloat16)
    back_rows = expert_sum.astype(jnp.bfloat16).reshape(ep_size, capacity, expert_sum.shape[1])
    returned = lax.all_to_all(back_rows, "ep", split_axis=0, concat_axis=0, tiled=True).reshape(
        ep_size * capacity, expert_sum.shape[1]
    )
    picked = returned[target].astype(jnp.float32).reshape(row_count, TOP, expert_sum.shape[1])
    expert_output = jnp.sum(picked * route_weight[:, :, None], axis=1).astype(jnp.bfloat16)
    return (mixer_output, expert_output)


def solution(mesh):
    return jax.shard_map(
        on_device,
        mesh=mesh,
        in_specs=(
            P("ep", "tp"),
            P("ep", "tp"),
            P(),
            P("tp"),
            P(None, "tp"),
            P(None, "tp"),
            P(),
            P("ep", None, "tp"),
            P("ep", None, "tp"),
            P("ep", None, "tp"),
            P("ep", None),
            P("ep", None),
        ),
        out_specs=(P("ep", "tp"), P("ep", "tp")),
        check_vma=False,
    )
```

profile of v0, /device:TPU:0, one launch (start us, length us, event | category | flops | bytes accessed | tf_op | source)
XLA Modules:
  0.0 316.2 jit_solution(4581051959690600166)
XLA Ops:
  7.2 1.0 copy.16
  8.6 0.7 broadcast_multiply_fusion.1
  9.3 2.3 reduce-window.6
  12.5 4.3 %scatter_custom_fusion = s32[1536]{0:T(1024)S(1)} fusion(s32[1024]{0:T(1024)S(1)} %bitcast.50, s32[1024]{0:T(1024)S(1)} %fusion.34, s32[]{:T(128)} %constant.78.clone.1), kind=kCustom, calls=%fused_computation.76 | custom fusion | bytes 6148 | tf_op jit(solution)/shard_map/scatter | solution.py:86
  16.9 5.4 %gather_fusion = bf16[1536,512]{1,0:T(8,128)(2,1)} fusion(bf16[512,512]{1,0:T(8,128)(2,1)S(1)} %copy-done.1, s32[2048]{0:T(1024)S(1)} %pad_clamp_fusion), kind=kCustom, calls=%fused_computation | custom fusion | bytes 3151872 | tf_op jit(solution)/shard_map/gather | solution.py:92
  22.3 1.7 broadcast_select_fusion
  24.0 44.1 %all_to_all.10 = bf16[8,192,512]{2,1,0:T(8,128)(2,1)} all-to-all(bf16[8,192,512]{2,1,0:T(8,128)(2,1)S(1)} %broadcast_select_fusion), channel_id=1, replica_groups=mesh['ep'=8,'tp'=4] {'ep'}, dimensions={0} | all-to-all | bytes 3145728 | tf_op jit(solution)/shard_map/all_to_all | solution.py:93
  68.2 0.7 all-gather.5.cloned.1.call-update
  68.9 68.2 %all-gather.9.cloned.1.call-done = bf16[1536,2048]{1,0:T(8,128)(2,1)} async-done(((bf16[1536,512]{1,0:T(8,128)(2,1)}), bf16[1536,2048]{1,0:T(8,128)(2,1)}) %all-gather.9.cloned.1.call-update) | async-done | bytes 6291472 | tf_op jit(solution)/shard_map/all_gather | solution.py:101
  137.1 3.8 %convert_reduce_fusion = f32[1536]{0:T(1024)S(1)} fusion(bf16[1536,2048]{1,0:T(8,128)(2,1)} %all-gather.9.cloned.1.call-done), kind=kLoop, calls=%fused_computation.4 | loop fusion | flops 6289920 | bytes 6297600 | tf_op jit(solution)/shard_map/reduce_sum | solution.py:28
  140.9 0.8 copy-done.2
  141.7 1.8 fusion.2
  143.5 2.4 fusion.4
  146.0 3.4 %convolution_bitcast_fusion.1 = f32[512,1536]{0,1:T(8,128)S(1)} fusion(bf16[1536,2048]{1,0:T(8,128)(2,1)S(1)} %fusion.4, bf16[1,2048,512]{2,1,0:T(8,128)(2,1)S(1)} %copy-done), kind=kOutput, calls=%fused_computation.19 | convolution fusion | flops 3221225472 | bytes 11534336 | tf_op jit(solution)/shard_map/dot_general | solution.py:108
  149.4 4.8 %fusion.11 = bf16[512,1536]{0,1:T(8,128)(2,1)} fusion(bf16[1536,2048]{1,0:T(8,128)(2,1)S(1)} %fusion.4, f32[512,1536]{0,1:T(8,128)S(1)} %convolution_bitcast_fusion.1, bf16[1,2048,512]{2,1,0:T(8,128)(2,1)S(1)} %copy-done.7), kind=kOutput, calls=%fused_computation.20 | convolution fusion | flops 3225944064 | bytes 13107200 | tf_op jit(solution)/shard_map/dot_general | solution.py:111
  154.5 19.4 %all-gather.5.cloned.1.call-done = bf16[512,2048]{1,0:T(8,128)(2,1)} async-done(((bf16[512,512]{1,0:T(8,128)(2,1)}), bf16[512,2048]{1,0:T(8,128)(2,1)}) %all-gather.5.cloned.1.call-update) | async-done | bytes 2097168 | tf_op jit(solution)/shard_map/all_gather | solution.py:90
  174.0 2.1 convert_reduce_fusion.1
  176.2 0.7 fusion.7
  176.9 1.3 fusion.23
  178.3 1.6 collective-permute-start
  179.9 1.3 collective-permute-start.1
  181.2 3.2 %collective-permute-done.1 = bf16[512,8]{0,1:T(8,128)(2,1)S(1)} collective-permute-done((bf16[512,8]{0,1:T(8,128)(2,1)S(1)}, bf16[512,8]{0,1:T(8,128)(2,1)S(1)}, u32[]{:S(2)}, u32[]{:S(2)}) %collective-permute-start.1) | collective-permute-done | bytes 8224 | tf_op jit(solution)/shard_map/ppermute | solution.py:21
  184.5 3.3 %fusion.30 = bf16[512,512]{0,1:T(8,128)(2,1)} fusion(bf16[512,512]{0,1:T(8,128)(2,1)S(1)} %fusion.23, f32[512,528]{0,1:T(8,128)S(1)} %maximum_convert_fusion, f32[512]{0:T(512)S(1)} %copy-done.6, f32[512]{0:T(512)S(1)} %get-tuple-element.4, f32[512]{0:T(512)S(1)} %get-tuple-element.5, f32[512]{0:T(512)S(1)} %get-tuple-element.6, ...), kind=kLoop, calls=%fused_computation.53 | loop fusion | flops 7077888 | bytes 17838080 | tf_op jit(solution)/shard_map/convert_element_type | solution.py:55
  187.8 57.9 %all-gather.11.cloned.1.call-done = bf16[2048,1536]{0,1:T(8,128)(2,1)} async-done(((bf16[512,1536]{0,1:T(8,128)(2,1)}), bf16[2048,1536]{0,1:T(8,128)(2,1)}) %all-gather.11.cloned.1.call-update) | async-done | bytes 6291472 | tf_op jit(solution)/shard_map/all_gather | solution.py:124
  245.8 8.1 %convolution_convert_fusion = bf16[1536,512]{1,0:T(8,128)(2,1)} fusion(bf16[2048,1536]{0,1:T(8,128)(2,1)} %all-gather.11.cloned.1.call-done, bf16[1,2048,512]{2,1,0:T(8,128)(2,1)} %param.21), kind=kOutput, calls=%fused_computation.21 | convolution fusion | flops 3222011904 | bytes 9961472 | tf_op jit(solution)/shard_map/dot_general | solution.py:123
  253.8 4.7 %all-to-all-start.1 = ((bf16[8,192,512]{2,1,0:T(8,128)(2,1)}), bf16[8,192,512]{2,1,0:T(8,128)(2,1)}, u32[]{:S(2)}, u32[]{:S(2)}) async-start(bf16[8,192,512]{2,1,0:T(8,128)(2,1)} %bitcast.48), calls=%async_computation.1 | async-start | bytes 3145728 | tf_op jit(solution)/shard_map/all_to_all | solution.py:131
  258.7 24.3 %all-gather.7.cloned.1.call-done = bf16[2048,512]{0,1:T(8,128)(2,1)} async-done(((bf16[512,512]{0,1:T(8,128)(2,1)}), bf16[2048,512]{0,1:T(8,128)(2,1)}) %all-gather.7.cloned.1.call-update) | async-done | bytes 2097168 | tf_op jit(solution)/shard_map/all_gather | solution.py:118
  283.1 4.3 %convolution_convert_fusion.1 = bf16[512,512]{1,0:T(8,128)(2,1)} fusion(bf16[2048,512]{0,1:T(8,128)(2,1)} %all-gather.7.cloned.1.call-done, bf16[2048,512]{1,0:T(8,128)(2,1)} %param.17), kind=kOutput, calls=%fused_computation.32 | convolution fusion | flops 1074003968 | bytes 4718592 | tf_op jit(solution)/shard_map/dot_general | solution.py:117
  287.4 9.1 %all-to-all-done.1 = bf16[8,192,512]{2,1,0:T(8,128)(2,1)} async-done(((bf16[8,192,512]{2,1,0:T(8,128)(2,1)}), bf16[8,192,512]{2,1,0:T(8,128)(2,1)}, u32[]{:S(2)}, u32[]{:S(2)}) %all-to-all-start.1) | async-done | bytes 1572896 | tf_op jit(solution)/shard_map/all_to_all | solution.py:131
  296.5 5.6 %gather_fusion.1 = bf16[1024,512]{1,0:T(8,128)(2,1)S(1)} fusion(bf16[1536,512]{1,0:T(8,128)(2,1)} %bitcast.12, s32[1024]{0:T(1024)S(1)} %broadcast_clamp_fusion), kind=kCustom, calls=%fused_computation.1 | custom fusion | bytes 2101248 | tf_op jit(solution)/shard_map/gather | solution.py:134
  302.1 2.4 reshape.168
  304.4 5.2 %multiply_reduce_fusion = bf16[512,512]{1,0:T(8,128)(2,1)} fusion(f32[512,2,512]{2,1,0:T(2,128)} %reshape.168, f32[512,2]{1,0:T(8,128)S(1)} %copy.18), kind=kLoop, calls=%fused_computation.26 | loop fusion | flops 786432 | bytes 2625536 | tf_op jit(solution)/shard_map/reduce_sum | solution.py:135
  (54 shorter events, 2.2 us)
Async XLA Ops:
  7.2 138.8 %copy-start = (bf16[1,2048,512]{2,1,0:T(8,128)(2,1)S(1)}, bf16[1,2048,512]{2,1,0:T(8,128)(2,1)}, u32[]{:S(2)}) copy-start(bf16[1,2048,512]{2,1,0:T(8,128)(2,1)} %param.19) | copy-start | bytes 6291460
  7.2 9.8 %copy-start.1 = (bf16[512,512]{1,0:T(8,128)(2,1)S(1)}, bf16[512,512]{1,0:T(8,128)(2,1)}, u32[]{:S(2)}) copy-start(bf16[512,512]{1,0:T(8,128)(2,1)} %param.13) | copy-start | bytes 1572868
  7.2 129.9 %all-gather.9.cloned.1.call-start = ((), (), s32[]{:S(2)}) async-start(), calls=%async_computation.4 | async-start | bytes 7864320 | tf_op jit(solution)/shard_map/all_gather | solution.py:101
  68.1 105.9 %all-gather.5.cloned.1.call-start = ((), (), s32[]{:S(2)}) async-start(), calls=%async_computation.2 | async-start | bytes 2621440 | tf_op jit(solution)/shard_map/all_gather | solution.py:90
  68.9 176.9 %all-gather.11.cloned.1.call-start = ((), (), s32[]{:S(2)}) async-start(), calls=%async_computation.5 | async-start | bytes 7864320 | tf_op jit(solution)/shard_map/all_gather | solution.py:124
  137.1 4.6 %copy-start.2 = (bf16[1536,2048]{1,0:T(8,128)(2,1)S(1)}, bf16[1536,2048]{1,0:T(8,128)(2,1)}, u32[]{:S(2)}) copy-start(bf16[1536,2048]{1,0:T(8,128)(2,1)} %all-gather.9.cloned.1.call-done) | copy-start | bytes 18874372
  141.7 1.8 copy-start.4
  145.9 3.5 %copy-start.7 = (bf16[1,2048,512]{2,1,0:T(8,128)(2,1)S(1)}, bf16[1,2048,512]{2,1,0:T(8,128)(2,1)}, u32[]{:S(2)}) copy-start(bf16[1,2048,512]{2,1,0:T(8,128)(2,1)} %param.20) | copy-start | bytes 6291460
  154.3 128.8 %all-gather.7.cloned.1.call-start = ((), (), s32[]{:S(2)}) async-start(), calls=%async_computation.3 | async-start | bytes 2621440 | tf_op jit(solution)/shard_map/all_gather | solution.py:118
  174.0 2.2 copy-start.3
  174.0 2.9 copy-start.8
  174.0 2.9 copy-start.9
  176.9 7.6 %copy-start.6 = (f32[512]{0:T(512)S(1)}, f32[512]{0:T(512)}, u32[]{:S(2)}) copy-start(f32[512]{0:T(512)} %param.15) | copy-start | bytes 6148
  178.3 2.9 collective-permute-start
  179.9 4.5 %collective-permute-start.1 = (bf16[512,8]{0,1:T(8,128)(2,1)S(1)}, bf16[512,8]{0,1:T(8,128)(2,1)S(1)}, u32[]{:S(2)}, u32[]{:S(2)}) collective-permute-start(bf16[512,8]{0,1:T(8,128)(2,1)S(1)} %get-tuple-element.3), channel_id=1, source_target_pairs={{4,0},{8,4},{12,8},{16,12},{20,16},{24,20},{28,24},{5,1},{9,5},{13... | collective-permute-start | bytes 24584 | tf_op jit(solution)/shard_map/ppermute | solution.py:21
  253.8 4.7 %copy-start.5 = (f32[512,2]{0,1:T(2,128)S(1)}, f32[512,2]{0,1:T(2,128)}, u32[]{:S(2)}) copy-start(f32[512,2]{0,1:T(2,128)} %param.23) | copy-start | bytes 12292
  253.8 42.6 %all-to-all-start.1 = ((bf16[8,192,512]{2,1,0:T(8,128)(2,1)}), bf16[8,192,512]{2,1,0:T(8,128)(2,1)}, u32[]{:S(2)}, u32[]{:S(2)}) async-start(bf16[8,192,512]{2,1,0:T(8,128)(2,1)} %bitcast.48), calls=%async_computation.1 | async-start | bytes 3145728 | tf_op jit(solution)/shard_map/all_to_all | solution.py:131
Sparse Core Ops, SparseCore 0:
  68.2 68.8 all-gather.8
  138.9 35.0 all-gather.4
  175.8 69.8 all-gather.10
  248.0 35.0 all-gather.6
where the time goes:
time: 317 us; the launch traced here: 316 us
  waiting for transfers between devices  183 us (58%)
  blocking collectives  44.1 us (14%)
  other arithmetic  24.5 us (8%)
  matrix products  21.9 us (7%)
  local copies, waits for them, and re-layouts  20.8 us (7%)
  between operations  14.1 us (4%)
  starting transfers between devices  7.95 us (3%)
    all_gather x1, waiting for transfers between devices, on_device(): lax.all_gather(slot_slices, 'tp', axis=1, tiled=True)  68.2 us
    all_gather x1, waiting for transfers between devices, on_device(): lax.all_gather(hidden_t, 'tp', axis=0, tiled=True)  57.9 us
    all_to_all x1, blocking collectives, on_device(): lax.all_to_all(outgoing.reshape(ep_size, capacity, feature_count), 'ep',...  44.1 us
    all_gather x1, waiting for transfers between devices, on_device(): lax.all_gather(pooled_t, 'tp', axis=0, tiled=True)  24.3 us
    all_gather x1, waiting for transfers between devices, on_device(): full_mix = lax.all_gather(mixer_rows, 'tp', axis=1, tiled=True)  19.4 us
    all_to_all x1, waiting for transfers between devices, on_device(): lax.all_to_all(back_rows, 'ep', split_axis=0, concat_axis=0, tiled=True)  9.13 us
    dot_general x1, matrix products, on_device(): lax.dot_general(lax.all_gather(hidden_t, 'tp', axis=0, tiled=True), down_...  8.08 us
  transfers between devices with their start and end apart: 7, of which 6 were waited for; matrix products, arithmetic and copies ran while one was open for 12% of the time, Pallas kernels for 0%

commit v1 on v0

--- a/solution.py
+++ b/solution.py
@@ -87,7 +87,19 @@
     )
     filled = (sender > 0)[:, None]
     source_row = jnp.maximum(sender - 1, 0)
-    full_mix = lax.all_gather(mixer_rows, "tp", axis=1, tiled=True)
+    world_n = jax.lax.axis_size("tp")
+    so_far_all = []
+    for j in range(1, world_n):
+        so_far_all.append((j - 1, j))
+    v_now = so_far_all + [(world_n - 1, 0)]
+    even = mixer_rows
+    rack = [even]
+    for _ in range(world_n - 1):
+        even = jax.lax.ppermute(even, "tp", v_now)
+        rack += [even]
+    now = jnp.concatenate([*reversed(rack)], 1)
+    carry = jax.lax.axis_index("tp")
+    full_mix = jnp.roll(now, (carry + 1) * even.shape[1], 1)
     feature_count = expert_rows.shape[1]
     outgoing = jnp.where(filled, expert_rows[source_row], jnp.zeros((), jnp.bfloat16))
     arrived = lax.all_to_all(

time: 317 us -> 314 us (level)
  waiting for transfers between devices: 183 us -> 174 us
  local copies, waits for them, and re-layouts: 20.8 us -> 25.4 us
  starting transfers between devices: 7.95 us -> 11.5 us
    ppermute x0 -> x3, waiting for transfers between devices: none -> 57.3 us  [on_device(): even = jax.lax.ppermute(even, 'tp', v_now)]
    all_gather x1, waiting for transfers between devices: 57.9 us -> 10.4 us  [on_device(): lax.all_gather(hidden_t, 'tp', axis=0, tiled=True)]
    all_gather x1 -> x0, waiting for transfers between devices: 19.4 us -> none  [on_device(): full_mix = lax.all_gather(mixer_rows, 'tp', axis=1, tiled=True)]
    unnamed x22 -> x29, local copies, waits for them, and re-layouts: 2.07 us -> 6.66 us
    ppermute x0 -> x3, starting transfers between devices: none -> 4.17 us  [on_device(): even = jax.lax.ppermute(even, 'tp', v_now)]
  transfers between devices with their start and end apart: 7 -> 9, of which waited for: 6 -> 8; matrix products, arithmetic and copies ran while one was open for 12% -> 7% of each run, Pallas kernels for 0% -> 0%
where the time goes in v1:
time: 314 us; the launch traced here: 313 us
  waiting for transfers between devices  174 us (55%)
  blocking collectives  44.1 us (14%)
  local copies, waits for them, and re-layouts  25.4 us (8%)
  other arithmetic  22.7 us (7%)
  matrix products  21.9 us (7%)
  between operations  14.1 us (4%)
  starting transfers between devices  11.5 us (4%)
    all_gather x1, waiting for transfers between devices, on_device(): lax.all_gather(slot_slices, 'tp', axis=1, tiled=True)  68.9 us
    ppermute x3, waiting for transfers between devices, on_device(): even = jax.lax.ppermute(even, 'tp', v_now)  57.3 us
    all_to_all x1, blocking collectives, on_device(): lax.all_to_all(outgoing.reshape(ep_size, capacity, feature_count), 'ep',...  44.1 us
    all_gather x1, waiting for transfers between devices, on_device(): lax.all_gather(pooled_t, 'tp', axis=0, tiled=True)  24.6 us
    all_gather x1, waiting for transfers between devices, on_device(): lax.all_gather(hidden_t, 'tp', axis=0, tiled=True)  10.4 us
    all_to_all x1, waiting for transfers between devices, on_device(): lax.all_to_all(back_rows, 'ep', split_axis=0, concat_axis=0, tiled=True)  8.83 us
    dot_general x1, matrix products, on_device(): lax.dot_general(lax.all_gather(hidden_t, 'tp', axis=0, tiled=True), down_...  8.08 us
    unnamed x29, local copies, waits for them, and re-layouts  6.66 us
  transfers between devices with their start and end apart: 9, of which 8 were waited for; matrix products, arithmetic and copies ran while one was open for 7% of the time, Pallas kernels for 0%

profile of v1, /device:TPU:0, one launch (start us, length us, event | category | flops | bytes accessed | tf_op | source)
XLA Modules:
  0.0 313.4 jit_solution(14929883607178266630)
XLA Ops:
  9.3 2.3 reduce-window.6
  12.5 4.3 %scatter_custom_fusion = s32[1536]{0:T(1024)S(1)} fusion(s32[1024]{0:T(1024)S(1)} %bitcast.50, s32[1024]{0:T(1024)S(1)} %fusion.35, s32[]{:T(128)} %constant.97.clone.1), kind=kCustom, calls=%fused_computation.85 | custom fusion | bytes 6148 | tf_op jit(solution)/shard_map/scatter | solution.py:86
  16.9 5.4 %gather_fusion = bf16[1536,512]{1,0:T(8,128)(2,1)} fusion(bf16[512,512]{1,0:T(8,128)(2,1)S(1)} %copy-done.1, s32[2048]{0:T(1024)S(1)} %pad_clamp_fusion), kind=kCustom, calls=%fused_computation | custom fusion | bytes 3151872 | tf_op jit(solution)/shard_map/gather | solution.py:104
  22.3 1.7 broadcast_select_fusion
  24.0 44.1 %all_to_all.10 = bf16[8,192,512]{2,1,0:T(8,128)(2,1)} all-to-all(bf16[8,192,512]{2,1,0:T(8,128)(2,1)S(1)} %broadcast_select_fusion), channel_id=1, replica_groups=mesh['ep'=8,'tp'=4] {'ep'}, dimensions={0} | all-to-all | bytes 3145728 | tf_op jit(solution)/shard_map/all_to_all | solution.py:105
  68.2 68.9 %all-gather.6.cloned.1.call-done = bf16[1536,2048]{1,0:T(8,128)(2,1)} async-done(((bf16[1536,512]{1,0:T(8,128)(2,1)}), bf16[1536,2048]{1,0:T(8,128)(2,1)}) %all-gather.6.cloned.1.call-update) | async-done | bytes 6291472 | tf_op jit(solution)/shard_map/all_gather | solution.py:113
  137.1 3.8 %convert_reduce_fusion = f32[1536]{0:T(1024)S(1)} fusion(bf16[1536,2048]{1,0:T(8,128)(2,1)} %all-gather.6.cloned.1.call-done), kind=kLoop, calls=%fused_computation.4 | loop fusion | flops 6289920 | bytes 6297600 | tf_op jit(solution)/shard_map/reduce_sum | solution.py:28
  141.7 1.8 fusion.2
  143.5 2.4 fusion.4
  146.0 3.4 %convolution_bitcast_fusion.1 = f32[512,1536]{0,1:T(8,128)S(1)} fusion(bf16[1536,2048]{1,0:T(8,128)(2,1)S(1)} %fusion.4, bf16[1,2048,512]{2,1,0:T(8,128)(2,1)S(1)} %copy-done), kind=kOutput, calls=%fused_computation.19 | convolution fusion | flops 3221225472 | bytes 11534336 | tf_op jit(solution)/shard_map/dot_general | solution.py:120
  149.4 4.8 %fusion.11 = bf16[512,1536]{0,1:T(8,128)(2,1)} fusion(bf16[1536,2048]{1,0:T(8,128)(2,1)S(1)} %fusion.4, f32[512,1536]{0,1:T(8,128)S(1)} %convolution_bitcast_fusion.1, bf16[1,2048,512]{2,1,0:T(8,128)(2,1)S(1)} %copy-done.7), kind=kOutput, calls=%fused_computation.20 | convolution fusion | flops 3225944064 | bytes 13107200 | tf_op jit(solution)/shard_map/dot_general | solution.py:123
  154.3 1.5 collective-permute-start
  155.8 16.7 %collective-permute-done = bf16[512,512]{1,0:T(8,128)(2,1)S(1)} collective-permute-done((bf16[512,512]{1,0:T(8,128)(2,1)S(1)}, bf16[512,512]{1,0:T(8,128)(2,1)S(1)}, u32[]{:S(2)}, u32[]{:S(2)}) %collective-permute-start) | collective-permute-done | bytes 524320 | tf_op jit(solution)/shard_map/ppermute | solution.py:98
  172.5 2.0 collective-permute-start.1
  174.5 22.4 %collective-permute-done.1 = bf16[512,512]{1,0:T(8,128)(2,1)} collective-permute-done((bf16[512,512]{1,0:T(8,128)(2,1)S(1)}, bf16[512,512]{1,0:T(8,128)(2,1)}, u32[]{:S(2)}, u32[]{:S(2)}) %collective-permute-start.1) | collective-permute-done | bytes 524320 | tf_op jit(solution)/shard_map/ppermute | solution.py:98
  197.6 18.2 %collective-permute-done.2 = bf16[512,512]{1,0:T(8,128)(2,1)} collective-permute-done((bf16[512,512]{1,0:T(8,128)(2,1)}, bf16[512,512]{1,0:T(8,128)(2,1)}, u32[]{:S(2)}, u32[]{:S(2)}) %collective-permute-start.2) | collective-permute-done | bytes 524320 | tf_op jit(solution)/shard_map/ppermute | solution.py:98
  217.0 1.1 constant_dynamic-update-slice_fusion.6
  218.2 1.2 constant_dynamic-update-slice_fusion.3
  221.8 1.3 fusion.24
  223.2 1.3 collective-permute-start.3
  224.5 1.3 collective-permute-start.4
  225.8 3.5 %collective-permute-done.4 = bf16[512,8]{0,1:T(8,128)(2,1)S(1)} collective-permute-done((bf16[512,8]{0,1:T(8,128)(2,1)S(1)}, bf16[512,8]{0,1:T(8,128)(2,1)S(1)}, u32[]{:S(2)}, u32[]{:S(2)}) %collective-permute-start.4) | collective-permute-done | bytes 8224 | tf_op jit(solution)/shard_map/ppermute | solution.py:21
  229.4 3.3 %fusion.31 = bf16[512,512]{0,1:T(8,128)(2,1)} fusion(bf16[512,512]{0,1:T(8,128)(2,1)S(1)} %fusion.24, f32[512,528]{0,1:T(8,128)S(1)} %maximum_convert_fusion, f32[512]{0:T(512)S(1)} %copy-done.6, f32[512]{0:T(512)S(1)} %get-tuple-element.4, f32[512]{0:T(512)S(1)} %get-tuple-element.5, f32[512]{0:T(512)S(1)} %get-tuple-element.6, ...), kind=kLoop, calls=%fused_computation.54 | loop fusion | flops 7077888 | bytes 17838080 | tf_op jit(solution)/shard_map/convert_element_type | solution.py:55
  232.7 10.4 %all-gather.8.cloned.1.call-done = bf16[2048,1536]{0,1:T(8,128)(2,1)} async-done(((bf16[512,1536]{0,1:T(8,128)(2,1)}), bf16[2048,1536]{0,1:T(8,128)(2,1)}) %all-gather.8.cloned.1.call-update) | async-done | bytes 6291472 | tf_op jit(solution)/shard_map/all_gather | solution.py:136
  243.1 8.1 %convolution_convert_fusion = bf16[1536,512]{1,0:T(8,128)(2,1)} fusion(bf16[2048,1536]{0,1:T(8,128)(2,1)} %all-gather.8.cloned.1.call-done, bf16[1,2048,512]{2,1,0:T(8,128)(2,1)} %param.21), kind=kOutput, calls=%fused_computation.21 | convolution fusion | flops 3222011904 | bytes 9961472 | tf_op jit(solution)/shard_map/dot_general | solution.py:135
  251.2 4.6 %all-to-all-start.1 = ((bf16[8,192,512]{2,1,0:T(8,128)(2,1)}), bf16[8,192,512]{2,1,0:T(8,128)(2,1)}, u32[]{:S(2)}, u32[]{:S(2)}) async-start(bf16[8,192,512]{2,1,0:T(8,128)(2,1)} %bitcast.48), calls=%async_computation.1 | async-start | bytes 3145728 | tf_op jit(solution)/shard_map/all_to_all | solution.py:143
  256.0 24.6 %all-gather.4.cloned.1.call-done = bf16[2048,512]{0,1:T(8,128)(2,1)} async-done(((bf16[512,512]{0,1:T(8,128)(2,1)}), bf16[2048,512]{0,1:T(8,128)(2,1)}) %all-gather.4.cloned.1.call-update) | async-done | bytes 2097168 | tf_op jit(solution)/shard_map/all_gather | solution.py:130
  280.6 4.3 %convolution_convert_fusion.1 = bf16[512,512]{1,0:T(8,128)(2,1)} fusion(bf16[2048,512]{0,1:T(8,128)(2,1)} %all-gather.4.cloned.1.call-done, bf16[2048,512]{1,0:T(8,128)(2,1)} %param.17), kind=kOutput, calls=%fused_computation.33 | convolution fusion | flops 1074003968 | bytes 4718592 | tf_op jit(solution)/shard_map/dot_general | solution.py:129
  284.9 8.8 %all-to-all-done.1 = bf16[8,192,512]{2,1,0:T(8,128)(2,1)} async-done(((bf16[8,192,512]{2,1,0:T(8,128)(2,1)}), bf16[8,192,512]{2,1,0:T(8,128)(2,1)}, u32[]{:S(2)}, u32[]{:S(2)}) %all-to-all-start.1) | async-done | bytes 1572896 | tf_op jit(solution)/shard_map/all_to_all | solution.py:143
  293.7 5.6 %gather_fusion.1 = bf16[1024,512]{1,0:T(8,128)(2,1)S(1)} fusion(bf16[1536,512]{1,0:T(8,128)(2,1)} %bitcast.12, s32[1024]{0:T(1024)S(1)} %broadcast_clamp_fusion), kind=kCustom, calls=%fused_computation.1 | custom fusion | bytes 2101248 | tf_op jit(solution)/shard_map/gather | solution.py:146
  299.3 2.4 reshape.168
  301.7 5.2 %multiply_reduce_fusion = bf16[512,512]{1,0:T(8,128)(2,1)} fusion(f32[512,2,512]{2,1,0:T(2,128)} %reshape.168, f32[512,2]{1,0:T(8,128)S(1)} %copy.18), kind=kLoop, calls=%fused_computation.26 | loop fusion | flops 786432 | bytes 2625536 | tf_op jit(solution)/shard_map/reduce_sum | solution.py:147
  (65 shorter events, 8.5 us)
Async XLA Ops:
  7.2 138.8 %copy-start = (bf16[1,2048,512]{2,1,0:T(8,128)(2,1)S(1)}, bf16[1,2048,512]{2,1,0:T(8,128)(2,1)}, u32[]{:S(2)}) copy-start(bf16[1,2048,512]{2,1,0:T(8,128)(2,1)} %param.19) | copy-start | bytes 6291460
  7.2 9.8 %copy-start.1 = (bf16[512,512]{1,0:T(8,128)(2,1)S(1)}, bf16[512,512]{1,0:T(8,128)(2,1)}, u32[]{:S(2)}) copy-start(bf16[512,512]{1,0:T(8,128)(2,1)} %param.13) | copy-start | bytes 1572868
  7.2 129.9 %all-gather.6.cloned.1.call-start = ((), (), s32[]{:S(2)}) async-start(), calls=%async_computation.3 | async-start | bytes 7864320 | tf_op jit(solution)/shard_map/all_gather | solution.py:113
  68.1 175.0 %all-gather.8.cloned.1.call-start = ((), (), s32[]{:S(2)}) async-start(), calls=%async_computation.4 | async-start | bytes 7864320 | tf_op jit(solution)/shard_map/all_gather | solution.py:136
  137.1 4.6 %copy-start.2 = (bf16[1536,2048]{1,0:T(8,128)(2,1)S(1)}, bf16[1536,2048]{1,0:T(8,128)(2,1)}, u32[]{:S(2)}) copy-start(bf16[1536,2048]{1,0:T(8,128)(2,1)} %all-gather.6.cloned.1.call-done) | copy-start | bytes 18874372
  140.9 2.6 copy-start.4
  145.9 3.5 %copy-start.7 = (bf16[1,2048,512]{2,1,0:T(8,128)(2,1)S(1)}, bf16[1,2048,512]{2,1,0:T(8,128)(2,1)}, u32[]{:S(2)}) copy-start(bf16[1,2048,512]{2,1,0:T(8,128)(2,1)} %param.20) | copy-start | bytes 6291460
  149.4 4.9 %copy-start.3 = (bf16[512,512]{1,0:T(8,128)(2,1)S(1)}, bf16[512,512]{1,0:T(8,128)(2,1)}, u32[]{:S(2)}) copy-start(bf16[512,512]{1,0:T(8,128)(2,1)} %param.12) | copy-start | bytes 1572868
  154.3 126.3 %all-gather.4.cloned.1.call-start = ((), (), s32[]{:S(2)}) async-start(), calls=%async_computation.2 | async-start | bytes 2621440 | tf_op jit(solution)/shard_map/all_gather | solution.py:130
  154.3 18.2 %collective-permute-start = (bf16[512,512]{1,0:T(8,128)(2,1)S(1)}, bf16[512,512]{1,0:T(8,128)(2,1)S(1)}, u32[]{:S(2)}, u32[]{:S(2)}) collective-permute-start(bf16[512,512]{1,0:T(8,128)(2,1)S(1)} %copy-done.3), channel_id=1, source_target_pairs={{0,1},{1,2},{2,3},{3,0},{4,5},{5,6},{6,7},{7,4},{8,9},{9,10},{10,1... | collective-permute-start | bytes 1572872 | tf_op jit(solution)/shard_map/ppermute | solution.py:98
  172.5 24.5 %collective-permute-start.1 = (bf16[512,512]{1,0:T(8,128)(2,1)S(1)}, bf16[512,512]{1,0:T(8,128)(2,1)}, u32[]{:S(2)}, u32[]{:S(2)}) collective-permute-start(bf16[512,512]{1,0:T(8,128)(2,1)S(1)} %collective-permute-done), channel_id=1, source_target_pairs={{0,1},{1,2},{2,3},{3,0},{4,5},{5,6},{6,7},{7,4},{8,9},{9,10},{10,1... | collective-permute-start | bytes 1572872 | tf_op jit(solution)/shard_map/ppermute | solution.py:98
  197.0 18.9 %collective-permute-start.2 = (bf16[512,512]{1,0:T(8,128)(2,1)}, bf16[512,512]{1,0:T(8,128)(2,1)}, u32[]{:S(2)}, u32[]{:S(2)}) collective-permute-start(bf16[512,512]{1,0:T(8,128)(2,1)} %collective-permute-done.1), channel_id=1, source_target_pairs={{0,1},{1,2},{2,3},{3,0},{4,5},{5,6},{6,7},{7,4},{8,9},{9,10},{10,1... | collective-permute-start | bytes 1572872 | tf_op jit(solution)/shard_map/ppermute | solution.py:98
  218.2 3.6 %copy-start.8 = (bf16[2048,512]{1,0:T(8,128)(2,1)S(1)}, bf16[2048,512]{1,0:T(8,128)(2,1)}, u32[]{:S(2)}) copy-start(bf16[2048,512]{1,0:T(8,128)(2,1)} %param.16) | copy-start | bytes 6291460
  218.2 3.6 %copy-start.9 = (f32[2048]{0:T(1024)S(1)}, f32[2048]{0:T(1024)}, u32[]{:S(2)}) copy-start(f32[2048]{0:T(1024)} %param.14) | copy-start | bytes 24580
  221.8 7.6 %copy-start.6 = (f32[512]{0:T(512)S(1)}, f32[512]{0:T(512)}, u32[]{:S(2)}) copy-start(f32[512]{0:T(512)} %param.15) | copy-start | bytes 6148
  223.2 2.6 collective-permute-start.3
  224.5 4.8 %collective-permute-start.4 = (bf16[512,8]{0,1:T(8,128)(2,1)S(1)}, bf16[512,8]{0,1:T(8,128)(2,1)S(1)}, u32[]{:S(2)}, u32[]{:S(2)}) collective-permute-start(bf16[512,8]{0,1:T(8,128)(2,1)S(1)} %get-tuple-element.3), channel_id=1, source_target_pairs={{4,0},{8,4},{12,8},{16,12},{20,16},{24,20},{28,24},{5,1},{9,5},{13... | collective-permute-start | bytes 24584 | tf_op jit(solution)/shard_map/ppermute | solution.py:21
  232.7 23.1 %copy-start.5 = (f32[512,2]{0,1:T(2,128)S(1)}, f32[512,2]{0,1:T(2,128)}, u32[]{:S(2)}) copy-start(f32[512,2]{0,1:T(2,128)} %param.23) | copy-start | bytes 12292
  251.2 42.5 %all-to-all-start.1 = ((bf16[8,192,512]{2,1,0:T(8,128)(2,1)}), bf16[8,192,512]{2,1,0:T(8,128)(2,1)}, u32[]{:S(2)}, u32[]{:S(2)}) async-start(bf16[8,192,512]{2,1,0:T(8,128)(2,1)} %bitcast.48), calls=%async_computation.1 | async-start | bytes 3145728 | tf_op jit(solution)/shard_map/all_to_all | solution.py:143
Sparse Core Ops, SparseCore 0:
  68.2 68.8 all-gather.5
  154.4 88.6 all-gather.7
  245.5 35.0 all-gather.3
